TPU v7x, 32 devices: a whole 2x2x4 slice. The times are simulated.
32 devices in a mesh: fs: 8 (over z, y), tp: 4 (over x, core).
Axes of the slice: x: 2, y: 2, z: 4, core: 2. Of those that a mesh axis runs over, the one named last changes fastest.
Arguments:
- tokens: bfloat16 [640, 3072], P('tp'), may hold values from -6 to 6
- gain_first: float32 [3072], replicated, may hold values from 0.1 to 1.9
- gain_second: float32 [3072], replicated, may hold values from 0.1 to 1.9
- gate_first: float32 [3072, 8192], P('fs', 'tp'), may hold values from -0.109375 to 0.109375
- up_first: float32 [3072, 8192], P('fs', 'tp'), may hold values from -0.109375 to 0.109375
- down_first: float32 [8192, 3072], P('fs', 'tp'), may hold values from -0.09375 to 0.09375
- gate_second: float32 [3072, 8192], P('fs', 'tp'), may hold values from -0.109375 to 0.109375
- up_second: float32 [3072, 8192], P('fs', 'tp'), may hold values from -0.109375 to 0.109375
- down_second: float32 [8192, 3072], P('fs', 'tp'), may hold values from -0.09375 to 0.09375
Outputs:
- result_rows: bfloat16 [640, 3072], P('tp')
- serve_gate_first: bfloat16 [3072, 8192], P(None, 'fs')
- serve_up_first: bfloat16 [3072, 8192], P(None, 'fs')
- serve_down_first: bfloat16 [8192, 3072], P('fs')
- serve_gate_second: bfloat16 [3072, 8192], P(None, 'fs')
- serve_up_second: bfloat16 [3072, 8192], P(None, 'fs')
- serve_down_second: bfloat16 [8192, 3072], P('fs')
All inputs are finite; a program needn't handle non-finite values.
Results may differ from a plain program's by a relative error of at most 0.011.
Values may be sent and summed in bfloat16 or wider, within the bound.
A program may use at most 192 MiB of HBM per device.

v0:
```python
import jax
import jax.numpy as jnp
from jax import lax
from jax.sharding import PartitionSpec as P


def plain_norm(values):
    values = values.astype(jnp.float32)
    center = jnp.mean(values, axis=-1, keepdims=True)
    spread = jnp.mean(jnp.square(values - center), axis=-1, keepdims=True)
    return (values - center) * lax.rsqrt(spread + 1e-05)


def sum_over_hidden(partial_value):
    pieces = lax.all_to_all(
        partial_value.astype(jnp.bfloat16), "fs", split_axis=1, concat_axis=0, tiled=True
    )
    rows = partial_value.shape[0]
    pieces = pieces.reshape(-1, rows, pieces.shape[1]).astype(jnp.float32)
    summed = jnp.sum(pieces, axis=0).astype(jnp.bfloat16)
    return lax.all_gather(summed, "fs", axis=1, tiled=True).astype(jnp.float32)


def regroup(folded):
    spread = lax.all_to_all(folded, "tp", split_axis=0, concat_axis=1, tiled=True)
    parts = lax.axis_size("fs")
    rows = spread.shape[0]
    owned = lax.all_to_all(spread, "fs", split_axis=1, concat_axis=0, tiled=True)
    owned = owned.reshape(parts, rows, owned.shape[1])
    whole = lax.all_gather(owned, "tp", axis=1, tiled=True)
    return whole.reshape(-1, whole.shape[2])


def half_step(normed, scales, w_gate, w_rising, w_down):
    gate_part = jnp.dot(normed, w_gate, preferred_element_type=jnp.float32)
    rising = jnp.dot(normed, w_rising, preferred_element_type=jnp.float32)
    hidden = (jax.nn.silu(gate_part) * rising).astype(jnp.bfloat16)
    partial_value = jnp.dot(hidden, w_down, preferred_element_type=jnp.float32)
    block = sum_over_hidden(partial_value)
    mixed = 1.6817928 * scales[None, :] * normed.astype(jnp.float32) + 0.5 * block
    return plain_norm(mixed).astype(jnp.bfloat16)


def on_device(
    tokens,
    gain_first,
    gain_second,
    gate_first,
    up_first,
    down_first,
    gate_second,
    up_second,
    down_second,
):
    row_count = gate_first.shape[0]
    offset = lax.axis_index("fs") * row_count

    def fold_gain(weight, scales):
        picked = lax.dynamic_slice_in_dim(scales, offset, row_count, 0)
        return (picked[:, None] * weight).astype(jnp.bfloat16)

    serve_gate_first = regroup(fold_gain(gate_first, gain_first))
    serve_up_first = regroup(fold_gain(up_first, gain_first))
    serve_down_first = lax.all_gather(down_first.astype(jnp.bfloat16), "tp", axis=1, tiled=True)
    serve_gate_second = regroup(fold_gain(gate_second, gain_second))
    serve_up_second = regroup(fold_gain(up_second, gain_second))
    serve_down_second = lax.all_gather(down_second.astype(jnp.bfloat16), "tp", axis=1, tiled=True)
    normed_zero = plain_norm(tokens).astype(jnp.bfloat16)
    normed_one = half_step(
        normed_zero, gain_first, serve_gate_first, serve_up_first, serve_down_first
    )
    result_rows = half_step(
        normed_one, gain_second, serve_gate_second, serve_up_second, serve_down_second
    )
    return (
        result_rows,
        serve_gate_first,
        serve_up_first,
        serve_down_first,
        serve_gate_second,
        serve_up_second,
        serve_down_second,
    )


def solution(mesh):
    placed = (
        P("tp", None),
        P(),
        P(),
        P("fs", "tp"),
        P("fs", "tp"),
        P("fs", "tp"),
        P("fs", "tp"),
        P("fs", "tp"),
        P("fs", "tp"),
    )
    return jax.shard_map(
        on_device,
        mesh=mesh,
        in_specs=placed,
        out_specs=(
            P("tp", None),
            P(None, "fs"),
            P(None, "fs"),
            P("fs", None),
            P(None, "fs"),
            P(None, "fs"),
            P("fs", None),
        ),
        check_vma=False,
    )
```

profile of v0, /device:TPU:0, one launch (start us, length us, event | category | flops | bytes accessed | tf_op | source)
XLA Modules:
  0.0 523.0 jit_solution(2696292961990616382)
XLA Ops:
  8.0 3.7 multiply_convert_fusion.3
  11.7 24.1 %all_to_all.154 = bf16[4,96,2048]{2,1,0:T(8,128)(2,1)S(1)} all-to-all(bf16[4,96,2048]{2,1,0:T(8,128)(2,1)S(1)} %bitcast.44), channel_id=1, replica_groups=mesh['fs'=8,'tp'=4] {'tp'}, dimensions={0} | all-to-all | bytes 3145728 | tf_op jit(solution)/shard_map/all_to_all | solution.py:25
  37.0 1.8 all_to_all.119
  38.9 2.3 copy.29
  41.2 42.3 %all_to_all.155 = bf16[96,8,1024]{2,0,1:T(8,128)(2,1)S(1)} all-to-all(bf16[96,8,1024]{2,0,1:T(8,128)(2,1)S(1)} %copy.29), channel_id=1, replica_groups=mesh['fs'=8,'tp'=4] {'fs'}, dimensions={1} | all-to-all | bytes 3145728 | tf_op jit(solution)/shard_map/all_to_all | solution.py:28
  83.5 2.0 copy.30
  85.6 36.1 %all_to_all.156 = bf16[4,96,2048]{2,1,0:T(8,128)(2,1)S(1)} all-to-all(bf16[4,96,2048]{2,1,0:T(8,128)(2,1)S(1)} %bitcast.42), channel_id=1, replica_groups=mesh['fs'=8,'tp'=4] {'tp'}, dimensions={0} | all-to-all | bytes 3145728 | tf_op jit(solution)/shard_map/all_to_all | solution.py:25
  124.2 39.1 %all_to_all.157 = bf16[96,8,1024]{2,0,1:T(8,128)(2,1)S(1)} all-to-all(bf16[96,8,1024]{2,0,1:T(8,128)(2,1)S(1)} %copy.33), channel_id=1, replica_groups=mesh['fs'=8,'tp'=4] {'fs'}, dimensions={1} | all-to-all | bytes 3145728 | tf_op jit(solution)/shard_map/all_to_all | solution.py:28
  163.3 2.0 copy.34
  166.8 3.9 multiply_convert_fusion.1
  170.7 39.8 %all_to_all.158 = bf16[4,96,2048]{2,1,0:T(8,128)(2,1)S(1)} all-to-all(bf16[4,96,2048]{2,1,0:T(8,128)(2,1)S(1)} %bitcast.45), channel_id=1, replica_groups=mesh['fs'=8,'tp'=4] {'tp'}, dimensions={0} | all-to-all | bytes 3145728 | tf_op jit(solution)/shard_map/all_to_all | solution.py:25
  211.7 1.8 all_to_all.133
  213.6 2.3 copy.38
  215.8 51.1 %all_to_all.159 = bf16[96,8,1024]{2,0,1:T(8,128)(2,1)S(1)} all-to-all(bf16[96,8,1024]{2,0,1:T(8,128)(2,1)S(1)} %copy.38), channel_id=1, replica_groups=mesh['fs'=8,'tp'=4] {'fs'}, dimensions={1} | all-to-all | bytes 3145728 | tf_op jit(solution)/shard_map/all_to_all | solution.py:28
  266.9 2.0 copy.39
  269.0 26.1 %all_to_all.160 = bf16[4,96,2048]{2,1,0:T(8,128)(2,1)S(1)} all-to-all(bf16[4,96,2048]{2,1,0:T(8,128)(2,1)S(1)} %bitcast.43), channel_id=1, replica_groups=mesh['fs'=8,'tp'=4] {'tp'}, dimensions={0} | all-to-all | bytes 3145728 | tf_op jit(solution)/shard_map/all_to_all | solution.py:25
  297.6 39.2 %all_to_all.161 = bf16[96,8,1024]{2,0,1:T(8,128)(2,1)S(1)} all-to-all(bf16[96,8,1024]{2,0,1:T(8,128)(2,1)S(1)} %copy.42), channel_id=1, replica_groups=mesh['fs'=8,'tp'=4] {'fs'}, dimensions={1} | all-to-all | bytes 3145728 | tf_op jit(solution)/shard_map/all_to_all | solution.py:28
  336.8 2.0 copy.43
  342.0 9.7 %copy.31 = bf16[8,384,1024]{2,1,0:T(8,128)(2,1)} copy(bf16[8,384,1024]{2,0,1:T(8,128)(2,1)} %all-gather.7.cloned.1.call-done) | data formatting | bytes 12582912 | tf_op jit(solution)/shard_map/all_gather | solution.py:30
  351.7 9.2 %copy.35 = bf16[8,384,1024]{2,1,0:T(8,128)(2,1)} copy(bf16[8,384,1024]{2,0,1:T(8,128)(2,1)} %all-gather.9.cloned.1.call-done) | data formatting | bytes 12582912 | tf_op jit(solution)/shard_map/all_gather | solution.py:30
  362.3 7.0 %convolution_convert_fusion.1 = bf16[160,3072]{1,0:T(8,128)(2,1)S(1)} fusion(bf16[1024,3072]{1,0:T(8,128)(2,1)} %all-gather.11.cloned.1.call-done, bf16[3072,1024]{1,0:T(8,128)(2,1)} %bitcast.38, f32[160,1024]{1,0:T(8,128)S(1)} %fusion.14, bf16[160,3072]{1,0:T(8,128)(2,1)S(1)} %copy-done.1, f32[160]{0:T(256)S(1)} %add_rsqrt_fusion.2, ...), kind=kOutput, calls=%fused_computation.1 | convolution fusion | flops 2016706560 | bytes 15205632 | tf_op jit(solution)/shard_map/dot_general | solution.py:38
  370.3 3.8 all-to-all-start.4
  374.1 9.1 %copy.40 = bf16[8,384,1024]{2,1,0:T(8,128)(2,1)} copy(bf16[8,384,1024]{2,0,1:T(8,128)(2,1)} %all-gather.13.cloned.1.call-done) | data formatting | bytes 12582912 | tf_op jit(solution)/shard_map/all_gather | solution.py:30
  383.7 9.0 %copy.44 = bf16[8,384,1024]{2,1,0:T(8,128)(2,1)} copy(bf16[8,384,1024]{2,0,1:T(8,128)(2,1)} %all-gather.15.cloned.1.call-done) | data formatting | bytes 12582912 | tf_op jit(solution)/shard_map/all_gather | solution.py:30
  392.7 5.5 %all-to-all-done.4 = bf16[160,8,384]{2,0,1:T(8,128)(2,1)S(1)} async-done(((bf16[160,8,384]{2,0,1:T(8,128)(2,1)}), bf16[160,8,384]{2,0,1:T(8,128)(2,1)S(1)}, u32[]{:S(2)}, u32[]{:S(2)}) %all-to-all-start.4) | async-done | bytes 983072 | tf_op jit(solution)/shard_map/all_to_all | solution.py:15
  398.3 33.7 %all_gather.27 = bf16[160,3072]{1,0:T(8,128)(2,1)S(1)} all-gather(bf16[160,384]{1,0:T(8,128)(2,1)S(1)} %reduce_sum.80), channel_id=1, replica_groups=mesh['fs'=8,'tp'=4] {'fs'}, dimensions={1}, use_global_device_ids=true | all-gather | bytes 1105920 | tf_op jit(solution)/shard_map/all_gather | solution.py:21
  436.0 6.9 %convolution_convert_fusion = bf16[160,3072]{1,0:T(8,128)(2,1)S(1)} fusion(bf16[1024,3072]{1,0:T(8,128)(2,1)} %all-gather.17.cloned.1.call-done, bf16[160,3072]{1,0:T(8,128)(2,1)S(1)} %multiply_convert_fusion.5, bf16[3072,1024]{1,0:T(8,128)(2,1)} %bitcast.40, f32[160,1024]{1,0:T(8,128)S(1)} %fusion.16), kind=kOutput, calls=%fused_computation | convolution fusion | flops 2014740480 | bytes 15204352 | tf_op jit(solution)/shard_map/dot_general | solution.py:38
  444.0 3.6 all-to-all-start.9
  447.6 23.0 %all-to-all-done.9 = bf16[160,8,384]{2,0,1:T(8,128)(2,1)S(1)} async-done(((bf16[160,8,384]{2,0,1:T(8,128)(2,1)}), bf16[160,8,384]{2,0,1:T(8,128)(2,1)S(1)}, u32[]{:S(2)}, u32[]{:S(2)}) %all-to-all-start.9) | async-done | bytes 983072 | tf_op jit(solution)/shard_map/all_to_all | solution.py:15
  470.6 33.6 %all_gather.31 = bf16[160,3072]{1,0:T(8,128)(2,1)S(1)} all-gather(bf16[160,384]{1,0:T(8,128)(2,1)S(1)} %reduce_sum.83), channel_id=1, replica_groups=mesh['fs'=8,'tp'=4] {'fs'}, dimensions={1}, use_global_device_ids=true | all-gather | bytes 1105920 | tf_op jit(solution)/shard_map/all_gather | solution.py:21
  506.9 6.1 %copy.54 = bf16[1024,3072]{1,0:T(8,128)(2,1)} copy(bf16[1024,3072]{1,0:T(8,128)(2,1)} %all-gather.11.cloned.1.call-done) | data formatting | bytes 12582912
  513.0 2.7 copy.55
  (71 shorter events, 23.9 us)
Async XLA Ops:
  7.2 334.9 %all-gather.7.cloned.1.call-start = ((), (), s32[]{:S(2)}) async-start(), calls=%async_computation.10 | async-start | bytes 7864320 | tf_op jit(solution)/shard_map/all_gather | solution.py:30
  85.5 266.2 %all-gather.9.cloned.1.call-start = ((), (), s32[]{:S(2)}) async-start(), calls=%async_computation.11 | async-start | bytes 7864320 | tf_op jit(solution)/shard_map/all_gather | solution.py:30
  163.3 2.1 copy-start.3
  165.3 1.4 copy-start.6
  165.3 196.9 %all-gather.11.cloned.1.call-start = ((), (), s32[]{:S(2)}) async-start(), calls=%async_computation.12 | async-start | bytes 7864320 | tf_op jit(solution)/shard_map/all_gather | solution.py:64
  166.7 207.4 %all-gather.13.cloned.1.call-start = ((), (), s32[]{:S(2)}) async-start(), calls=%async_computation.13 | async-start | bytes 7864320 | tf_op jit(solution)/shard_map/all_gather | solution.py:30
  269.0 114.7 %all-gather.15.cloned.1.call-start = ((), (), s32[]{:S(2)}) async-start(), calls=%async_computation.14 | async-start | bytes 7864320 | tf_op jit(solution)/shard_map/all_gather | solution.py:30
  336.8 2.1 copy-start.4
  338.8 97.2 %all-gather.17.cloned.1.call-start = ((), (), s32[]{:S(2)}) async-start(), calls=%async_computation.15 | async-start | bytes 7864320 | tf_op jit(solution)/shard_map/all_gather | solution.py:67
  340.2 1.2 copy-start.1
  351.7 9.2 %copy-start.2 = (bf16[8,384,1024]{2,1,0:T(8,128)(2,1)S(1)}, bf16[8,384,1024]{2,1,0:T(8,128)(2,1)}, u32[]{:S(2)}) copy-start(bf16[8,384,1024]{2,1,0:T(8,128)(2,1)} %copy.31) | copy-start | bytes 18874372
  369.3 4.8 copy-start.5
  370.3 27.8 %all-to-all-start.4 = ((bf16[160,8,384]{2,0,1:T(8,128)(2,1)}), bf16[160,8,384]{2,0,1:T(8,128)(2,1)S(1)}, u32[]{:S(2)}, u32[]{:S(2)}) async-start(bf16[160,8,384]{2,0,1:T(8,128)(2,1)} %bitcast.31), calls=%async_computation.4 | async-start | bytes 1966080 | tf_op jit(solution)/shard_map/all_to_all | solution.py:15
  432.0 2.8 copy-start
  444.0 26.5 %all-to-all-start.9 = ((bf16[160,8,384]{2,0,1:T(8,128)(2,1)}), bf16[160,8,384]{2,0,1:T(8,128)(2,1)S(1)}, u32[]{:S(2)}, u32[]{:S(2)}) async-start(bf16[160,8,384]{2,0,1:T(8,128)(2,1)} %bitcast.30), calls=%async_computation.9 | async-start | bytes 1966080 | tf_op jit(solution)/shard_map/all_to_all | solution.py:15
  505.4 7.6 %slice-start = ((s8[6291456]{0:T(1024)(128)(4,1)}), s8[4194304]{0:T(1024)(128)(4,1)S(1)}, s32[]{:S(2)}) async-start(s8[6291456]{0:T(1024)(128)(4,1)} %bitcast.34), calls=%async_computation.16 | async-start | bytes 8388608
  506.9 6.1 %slice-start.1 = ((s8[6291456]{0:T(1024)(128)(4,1)}), s8[2097152]{0:T(1024)(128)(4,1)S(1)}, s32[]{:S(2)}) async-start(s8[6291456]{0:T(1024)(128)(4,1)} %bitcast.34), calls=%async_computation.17 | async-start | bytes 4194304
Sparse Core Ops, SparseCore 0:
  85.6 57.7 all-gather.6
  165.4 61.2 all-gather.8
  228.8 46.1 all-gather.10
  276.5 50.4 all-gather.12
  338.9 44.6 all-gather.14
  385.7 46.3 all-gather.16
where the time goes:
time: 532 us; the launch traced here: 523 us
  blocking collectives  365 us (69%)
  local copies, waits for them, and re-layouts  74 us (14%)
  waiting for transfers between devices  29.1 us (5%)
  matrix products  16.4 us (3%)
  other arithmetic  16.1 us (3%)
  between operations  14.8 us (3%)
  starting transfers between devices  7.57 us (1%)
    all_to_all x4, blocking collectives, regroup(): lax.all_to_all(spread, 'fs', split_axis=1, concat_axis=0, tiled=True)  172 us
    all_to_all x4, blocking collectives, regroup(): lax.all_to_all(folded, 'tp', split_axis=0, concat_axis=1, tiled=True)  126 us
    all_gather x2, blocking collectives, sum_over_hidden(): return lax.all_gather(summed, 'fs', axis=1, tiled=True).astype(jnp.float32)  67.3 us
    all_gather x4, local copies, waits for them, and re-layouts, regroup(): whole = lax.all_gather(owned, 'tp', axis=1, tiled=True)  36.9 us
    all_to_all x2, waiting for transfers between devices, sum_over_hidden(): lax.all_to_all(partial_value.astype(jnp.bfloat16), 'fs', split_axis=1, co...  28.4 us
    all_to_all x12, local copies, waits for them, and re-layouts, regroup(): lax.all_to_all(spread, 'fs', split_axis=1, concat_axis=0, tiled=True)  18.8 us
    dot_general x2, matrix products, half_step(): partial_value = jnp.dot(hidden, w_down, preferred_element_type=jnp.float32)  13.9 us
  transfers between devices with their start and end apart: 8, of which 3 were waited for; matrix products, arithmetic and copies ran while one was open for 14% of the time, Pallas kernels for 0%

commit v1 on v0

--- a/solution.py
+++ b/solution.py
@@ -25,7 +25,10 @@
     spread = lax.all_to_all(folded, "tp", split_axis=0, concat_axis=1, tiled=True)
     parts = lax.axis_size("fs")
     rows = spread.shape[0]
-    owned = lax.all_to_all(spread, "fs", split_axis=1, concat_axis=0, tiled=True)
+    owned = jnp.concatenate(
+        lax.all_to_all(jnp.stack(jnp.split(spread, lax.axis_size("fs"), axis=1)), "fs", 0, 0),
+        axis=0,
+    )
     owned = owned.reshape(parts, rows, owned.shape[1])
     whole = lax.all_gather(owned, "tp", axis=1, tiled=True)
     return whole.reshape(-1, whole.shape[2])

time: 532 us -> 508 us (0.955); the launches traced: 523 us -> 507 us
  local copies, waits for them, and re-layouts: 74 us -> 32.2 us
  waiting for transfers between devices: 29.1 us -> 49.1 us
  matrix products: 16.4 us -> 22 us
    all_gather x4 -> x0, local copies, waits for them, and re-layouts: 36.9 us -> none  [regroup(): whole = lax.all_gather(owned, 'tp', axis=1, tiled=True)]
    all_to_all x2, waiting for transfers between devices: 28.4 us -> 48.9 us  [sum_over_hidden(): lax.all_to_all(partial_value.astype(jnp.bfloat16), 'fs', split_axis=1, co...]
    all_to_all x12 -> x0, local copies, waits for them, and re-layouts: 18.8 us -> none  [regroup(): lax.all_to_all(spread, 'fs', split_axis=1, concat_axis=0, tiled=True)]
    unnamed x20 -> x60, local copies, waits for them, and re-layouts: 10.4 us -> 28.6 us
    all_to_all x4, blocking collectives: 172 us -> 165 us  [regroup(): lax.all_to_all(jnp.stack(jnp.split(spread, lax.axis_size('fs'), axis=1)),...]
    dot_general x2, matrix products: 2.55 us -> 8.05 us  [half_step(): gate_part = jnp.dot(normed, w_gate, preferred_element_type=jnp.float32)]
  transfers between devices with their start and end apart: 8 -> 8, of which waited for: 3 -> 2; matrix products, arithmetic and copies ran while one was open for 14% -> 6% of each run, Pallas kernels for 0% -> 0%
where the time goes in v1:
time: 508 us; the launch traced here: 507 us
  blocking collectives  361 us (71%)
  waiting for transfers between devices  49.1 us (10%)
  local copies, waits for them, and re-layouts  32.2 us (6%)
  matrix products  22 us (4%)
  other arithmetic  19.7 us (4%)
  between operations  14.6 us (3%)
  starting transfers between devices  8.66 us (2%)
    all_to_all x4, blocking collectives, regroup(): lax.all_to_all(jnp.stack(jnp.split(spread, lax.axis_size('fs'), axis=1)),...  165 us
    all_to_all x4, blocking collectives, regroup(): lax.all_to_all(folded, 'tp', split_axis=0, concat_axis=1, tiled=True)  130 us
    all_gather x2, blocking collectives, sum_over_hidden(): return lax.all_gather(summed, 'fs', axis=1, tiled=True).astype(jnp.float32)  66.2 us
    all_to_all x2, waiting for transfers between devices, sum_over_hidden(): lax.all_to_all(partial_value.astype(jnp.bfloat16), 'fs', split_axis=1, co...  48.9 us
    unnamed x60, local copies, waits for them, and re-layouts  28.6 us
    dot_general x2, matrix products, half_step(): partial_value = jnp.dot(hidden, w_down, preferred_element_type=jnp.float32)  14 us
  transfers between devices with their start and end apart: 8, of which 2 were waited for; matrix products, arithmetic and copies ran while one was open for 6% of the time, Pallas kernels for 0%

profile of v1, /device:TPU:0, one launch (start us, length us, event | category | flops | bytes accessed | tf_op | source)
XLA Modules:
  0.0 507.1 jit_solution(17659746832396600493)
XLA Ops:
  8.0 3.7 multiply_convert_fusion.3
  11.7 24.1 %all_to_all.122 = bf16[4,96,2048]{2,1,0:T(8,128)(2,1)S(1)} all-to-all(bf16[4,96,2048]{2,1,0:T(8,128)(2,1)S(1)} %bitcast.216), channel_id=1, replica_groups=mesh['fs'=8,'tp'=4] {'tp'}, dimensions={0} | all-to-all | bytes 3145728 | tf_op jit(solution)/shard_map/all_to_all | solution.py:25
  36.2 42.4 %all_to_all.123 = bf16[8,96,1024]{2,1,0:T(8,128)(2,1)} all-to-all(bf16[8,96,1024]{2,1,0:T(8,128)(2,1)S(1)} %fusion.34), channel_id=1, replica_groups=mesh['fs'=8,'tp'=4] {'fs'}, dimensions={0} | all-to-all | bytes 3145728 | tf_op jit(solution)/shard_map/all_to_all | solution.py:29
  78.7 3.2 convert_element_type.64
  81.9 39.3 %all_to_all.124 = bf16[4,96,2048]{2,1,0:T(8,128)(2,1)S(1)} all-to-all(bf16[4,96,2048]{2,1,0:T(8,128)(2,1)S(1)} %bitcast.182), channel_id=1, replica_groups=mesh['fs'=8,'tp'=4] {'tp'}, dimensions={0} | all-to-all | bytes 3145728 | tf_op jit(solution)/shard_map/all_to_all | solution.py:25
  121.6 39.8 %all_to_all.125 = bf16[8,96,1024]{2,1,0:T(8,128)(2,1)} all-to-all(bf16[8,96,1024]{2,1,0:T(8,128)(2,1)S(1)} %fusion.26), channel_id=1, replica_groups=mesh['fs'=8,'tp'=4] {'fs'}, dimensions={0} | all-to-all | bytes 3145728 | tf_op jit(solution)/shard_map/all_to_all | solution.py:29
  162.2 3.7 multiply_convert_fusion.1
  165.9 35.6 %all_to_all.126 = bf16[4,96,2048]{2,1,0:T(8,128)(2,1)S(1)} all-to-all(bf16[4,96,2048]{2,1,0:T(8,128)(2,1)S(1)} %bitcast.217), channel_id=1, replica_groups=mesh['fs'=8,'tp'=4] {'tp'}, dimensions={0} | all-to-all | bytes 3145728 | tf_op jit(solution)/shard_map/all_to_all | solution.py:25
  201.9 42.5 %all_to_all.127 = bf16[8,96,1024]{2,1,0:T(8,128)(2,1)} all-to-all(bf16[8,96,1024]{2,1,0:T(8,128)(2,1)S(1)} %fusion.18), channel_id=1, replica_groups=mesh['fs'=8,'tp'=4] {'fs'}, dimensions={0} | all-to-all | bytes 3145728 | tf_op jit(solution)/shard_map/all_to_all | solution.py:29
  244.5 3.3 convert_element_type.72
  247.8 31.0 %all_to_all.128 = bf16[4,96,2048]{2,1,0:T(8,128)(2,1)S(1)} all-to-all(bf16[4,96,2048]{2,1,0:T(8,128)(2,1)S(1)} %bitcast.183), channel_id=1, replica_groups=mesh['fs'=8,'tp'=4] {'tp'}, dimensions={0} | all-to-all | bytes 3145728 | tf_op jit(solution)/shard_map/all_to_all | solution.py:25
  279.1 39.8 %all_to_all.129 = bf16[8,96,1024]{2,1,0:T(8,128)(2,1)} all-to-all(bf16[8,96,1024]{2,1,0:T(8,128)(2,1)S(1)} %fusion.10), channel_id=1, replica_groups=mesh['fs'=8,'tp'=4] {'fs'}, dimensions={0} | all-to-all | bytes 3145728 | tf_op jit(solution)/shard_map/all_to_all | solution.py:29
  318.9 1.2 copy-done
  320.8 4.1 fusion.46
  324.9 7.1 %convolution_convert_fusion.1 = bf16[160,3072]{1,0:T(8,128)(2,1)S(1)} fusion(bf16[1024,3072]{1,0:T(8,128)(2,1)} %all-gather.11.cloned.1.call-done, bf16[3072,1024]{1,0:T(8,128)(2,1)} %bitcast.172, f32[160,1024]{1,0:T(8,128)S(1)} %fusion.46, bf16[160,3072]{1,0:T(8,128)(2,1)S(1)} %copy-done, f32[160]{0:T(256)S(1)} %add_rsqrt_fusion.2, ...), kind=kOutput, calls=%fused_computation.1 | convolution fusion | flops 2016706560 | bytes 15205632 | tf_op jit(solution)/shard_map/dot_general | solution.py:41
  333.1 3.6 all-to-all-start.4
  336.7 24.1 %all-to-all-done.4 = bf16[160,8,384]{2,0,1:T(8,128)(2,1)S(1)} async-done(((bf16[160,8,384]{2,0,1:T(8,128)(2,1)}), bf16[160,8,384]{2,0,1:T(8,128)(2,1)S(1)}, u32[]{:S(2)}, u32[]{:S(2)}) %all-to-all-start.4) | async-done | bytes 983072 | tf_op jit(solution)/shard_map/all_to_all | solution.py:15
  360.9 33.3 %all_gather.27 = bf16[160,3072]{1,0:T(8,128)(2,1)S(1)} all-gather(bf16[160,384]{1,0:T(8,128)(2,1)S(1)} %reduce_sum.80), channel_id=1, replica_groups=mesh['fs'=8,'tp'=4] {'fs'}, dimensions={1}, use_global_device_ids=true | all-gather | bytes 1105920 | tf_op jit(solution)/shard_map/all_gather | solution.py:21
  396.6 4.0 fusion.48
  400.6 6.9 %convolution_convert_fusion = bf16[160,3072]{1,0:T(8,128)(2,1)S(1)} fusion(bf16[1024,3072]{1,0:T(8,128)(2,1)} %all-gather.17.cloned.1.call-done, bf16[160,3072]{1,0:T(8,128)(2,1)S(1)} %multiply_convert_fusion.5, bf16[3072,1024]{1,0:T(8,128)(2,1)} %bitcast.178, f32[160,1024]{1,0:T(8,128)S(1)} %fusion.48), kind=kOutput, calls=%fused_computation | convolution fusion | flops 2014740480 | bytes 15204352 | tf_op jit(solution)/shard_map/dot_general | solution.py:41
  408.6 4.9 all-to-all-start.9
  413.4 24.8 %all-to-all-done.9 = bf16[160,8,384]{2,0,1:T(8,128)(2,1)S(1)} async-done(((bf16[160,8,384]{2,0,1:T(8,128)(2,1)}), bf16[160,8,384]{2,0,1:T(8,128)(2,1)S(1)}, u32[]{:S(2)}, u32[]{:S(2)}) %all-to-all-start.9) | async-done | bytes 983072 | tf_op jit(solution)/shard_map/all_to_all | solution.py:15
  438.3 33.0 %all_gather.31 = bf16[160,3072]{1,0:T(8,128)(2,1)S(1)} all-gather(bf16[160,384]{1,0:T(8,128)(2,1)S(1)} %reduce_sum.83), channel_id=1, replica_groups=mesh['fs'=8,'tp'=4] {'fs'}, dimensions={1}, use_global_device_ids=true | all-gather | bytes 1105920 | tf_op jit(solution)/shard_map/all_gather | solution.py:21
  472.4 1.5 multiply_convert_fusion.4
  473.9 6.4 %copy.70 = bf16[3072,1024]{1,0:T(8,128)(2,1)} copy(bf16[3072,1024]{1,0:T(8,128)(2,1)} %bitcast.169) | data formatting | bytes 12582912
  480.3 3.2 copy.71
  483.5 3.2 copy.72
  488.4 3.2 copy.73
  491.6 1.4 slice-done.9
  493.0 3.2 copy.74
  496.2 1.4 slice-done.7
  497.6 2.7 copy.75
  (103 shorter events, 11.2 us)
Async XLA Ops:
  7.2 313.6 %all-gather.7.cloned.1.call-start = ((), (), s32[]{:S(2)}) async-start(), calls=%async_computation.10 | async-start | bytes 7864320 | tf_op jit(solution)/shard_map/all_gather | solution.py:33
  78.6 246.3 %all-gather.11.cloned.1.call-start = ((), (), s32[]{:S(2)}) async-start(), calls=%async_computation.12 | async-start | bytes 7864320 | tf_op jit(solution)/shard_map/all_gather | solution.py:67
  81.9 243.0 %all-gather.9.cloned.1.call-start = ((), (), s32[]{:S(2)}) async-start(), calls=%async_computation.11 | async-start | bytes 7864320 | tf_op jit(solution)/shard_map/all_gather | solution.py:33
  161.4 0.7 copy-start.2
  161.4 235.2 %all-gather.13.cloned.1.call-start = ((), (), s32[]{:S(2)}) async-start(), calls=%async_computation.13 | async-start | bytes 7864320 | tf_op jit(solution)/shard_map/all_gather | solution.py:33
  244.4 156.2 %all-gather.17.cloned.1.call-start = ((), (), s32[]{:S(2)}) async-start(), calls=%async_computation.15 | async-start | bytes 7864320 | tf_op jit(solution)/shard_map/all_gather | solution.py:70
  247.8 152.8 %all-gather.15.cloned.1.call-start = ((), (), s32[]{:S(2)}) async-start(), calls=%async_computation.14 | async-start | bytes 7864320 | tf_op jit(solution)/shard_map/all_gather | solution.py:33
  318.9 1.2 copy-start
  332.0 4.6 copy-start.1
  333.1 27.7 %all-to-all-start.4 = ((bf16[160,8,384]{2,0,1:T(8,128)(2,1)}), bf16[160,8,384]{2,0,1:T(8,128)(2,1)S(1)}, u32[]{:S(2)}, u32[]{:S(2)}) async-start(bf16[160,8,384]{2,0,1:T(8,128)(2,1)} %bitcast.163), calls=%async_computation.4 | async-start | bytes 1966080 | tf_op jit(solution)/shard_map/all_to_all | solution.py:15
  408.6 29.6 %all-to-all-start.9 = ((bf16[160,8,384]{2,0,1:T(8,128)(2,1)}), bf16[160,8,384]{2,0,1:T(8,128)(2,1)S(1)}, u32[]{:S(2)}, u32[]{:S(2)}) async-start(bf16[160,8,384]{2,0,1:T(8,128)(2,1)} %bitcast.162), calls=%async_computation.9 | async-start | bytes 1966080 | tf_op jit(solution)/shard_map/all_to_all | solution.py:15
  472.4 7.9 %slice-start.4 = ((s8[6291456]{0:T(1024)(128)(4,1)}), s8[4194304]{0:T(1024)(128)(4,1)S(1)}, s32[]{:S(2)}) async-start(s8[6291456]{0:T(1024)(128)(4,1)} %bitcast.173), calls=%async_computation.20 | async-start | bytes 8388608
  473.9 6.4 %slice-start.5 = ((s8[6291456]{0:T(1024)(128)(4,1)}), s8[2097152]{0:T(1024)(128)(4,1)S(1)}, s32[]{:S(2)}) async-start(s8[6291456]{0:T(1024)(128)(4,1)} %bitcast.173), calls=%async_computation.21 | async-start | bytes 4194304
  473.9 9.6 %slice-start.2 = ((s8[6291456]{0:T(1024)(128)(4,1)}), s8[4194304]{0:T(1024)(128)(4,1)S(1)}, s32[]{:S(2)}) async-start(s8[6291456]{0:T(1024)(128)(4,1)} %bitcast.170), calls=%async_computation.18 | async-start | bytes 8388608
  480.3 3.2 slice-start.3
  480.3 7.2 %slice-start = ((s8[6291456]{0:T(1024)(128)(4,1)}), s8[4194304]{0:T(1024)(128)(4,1)S(1)}, s32[]{:S(2)}) async-start(s8[6291456]{0:T(1024)(128)(4,1)} %bitcast.165), calls=%async_computation.16 | async-start | bytes 8388608
  483.5 4.8 slice-start.1
  483.5 8.0 %slice-start.8 = ((s8[6291456]{0:T(1024)(128)(4,1)}), s8[2097152]{0:T(1024)(128)(4,1)S(1)}, s32[]{:S(2)}) async-start(s8[6291456]{0:T(1024)(128)(4,1)} %bitcast.179), calls=%async_computation.24 | async-start | bytes 4194304
  488.4 4.6 slice-start.9
  488.4 7.8 %slice-start.6 = ((s8[6291456]{0:T(1024)(128)(4,1)}), s8[2097152]{0:T(1024)(128)(4,1)S(1)}, s32[]{:S(2)}) async-start(s8[6291456]{0:T(1024)(128)(4,1)} %bitcast.176), calls=%async_computation.22 | async-start | bytes 4194304
  493.0 4.6 slice-start.7
Sparse Core Ops, SparseCore 0:
  78.7 61.0 all-gather.6
  142.0 57.5 all-gather.10
  201.1 48.5 all-gather.8
  251.2 54.4 all-gather.12
  307.7 44.3 all-gather.16
  353.6 46.3 all-gather.14
